TPU v7x, 32 devices: a whole 2x2x4 slice. The times are simulated.
32 devices in a mesh: ep: 16 (over z, x, core), tp: 2 (over y).
Axes of the slice: x: 2, y: 2, z: 4, core: 2. Of those that a mesh axis runs over, the one named last changes fastest.
Arguments:
- tokens: bfloat16 [256, 1024], P('ep'), may hold values from -6 to 6
- state: float32 [256, 16, 64, 64], P('ep', 'tp'), may hold values from -6 to 6
- w_recep: bfloat16 [1024, 1024], P(None, 'tp'), may hold values from -0.1875 to 0.1875
- w_key: bfloat16 [1024, 1024], P(None, 'tp'), may hold values from -0.1875 to 0.1875
- w_value: bfloat16 [1024, 1024], P(None, 'tp'), may hold values from -0.1875 to 0.1875
- w_out: bfloat16 [1024, 1024], P('tp'), may hold values from -0.1875 to 0.1875
- decay_base: float32 [1024], P('tp'), may hold values from -5 to 1
- decay_down: bfloat16 [1024, 64], replicated, may hold values from -0.1875 to 0.1875
- decay_up: bfloat16 [64, 1024], P(None, 'tp'), may hold values from -1 to 1
- rate_base: float32 [1024], P('tp'), may hold values from -4 to 4
- rate_down: bfloat16 [1024, 64], replicated, may hold values from -0.1875 to 0.1875
- rate_up: bfloat16 [64, 1024], P(None, 'tp'), may hold values from -1 to 1
- head_gain: float32 [1024], P('tp'), may hold values from 0.1 to 1.9
- first_gain: float32 [1024], replicated, may hold values from 0.2 to 4.8
- expert_gate: bfloat16 [16, 1024, 1408], P('ep', None, 'tp'), may hold values from -0.1875 to 0.1875
- expert_up: bfloat16 [16, 1024, 1408], P('ep', None, 'tp'), may hold values from -0.1875 to 0.1875
- expert_down: bfloat16 [16, 1408, 1024], P('ep', 'tp'), may hold values from -0.078125 to 0.078125
- dense_gate: bfloat16 [2816, 1024], P('ep'), may hold values from -0.1875 to 0.1875
- dense_up: bfloat16 [2816, 1024], P('ep'), may hold values from -0.1875 to 0.1875
- dense_down: bfloat16 [2816, 1024], P('ep', 'tp'), may hold values from -0.21875 to 0.21875
- branch_gate: bfloat16 [1024], replicated, may hold values from -0.1875 to 0.1875
- second_gain: float32 [1024], P('tp'), may hold values from 0.1 to 1.9
- routes: int32 [256, 2], P('ep'), may hold values from 0 to 3, all different within a row; in each aligned block of 16 rows (0 to 15, 16 to 31, ...) at most 16 rows name the same one
- route_weights: float32 [256, 2], P('ep'), may hold values from 0.2 to 1
Outputs:
- layer_output: bfloat16 [256, 1024], P('ep', 'tp')
Inputs may be any that keep to these rules, and one draw needn't show every extreme that they name: `routes`: each row names 2 different experts. In each aligned block of 16 rows no expert is named by more than 16 rows, a bound that some block reaches.
All inputs are finite; a program needn't handle non-finite values.
Results may differ from a plain program's by a relative error of at most 0.018.
Values may be sent and summed in bfloat16 or wider, within the bound.
A program may use at most 64 MiB of HBM per device.

v0:
```python
import jax
import jax.numpy as jnp
from jax import lax
from jax.sharding import PartitionSpec as P

SPLIT = 4
residual_scale = 1.4142135623730951
norm_epsilon = 1e-05
head_epsilon = 0.00064
key_epsilon = 1e-06


def time_mixer(
    tokens,
    state,
    w_recep,
    w_key,
    w_value,
    w_out,
    decay_base,
    decay_down,
    decay_up,
    rate_base,
    rate_down,
    rate_up,
    head_gain,
):
    row_count = tokens.shape[0]
    head_count = state.shape[1]
    head_size = state.shape[3]
    recep = jnp.dot(tokens, w_recep, preferred_element_type=jnp.float32).reshape(
        row_count, head_count, head_size
    )
    key_vecs = jnp.dot(tokens, w_key, preferred_element_type=jnp.float32).reshape(
        row_count, head_count, head_size
    )
    value_vecs = jnp.dot(tokens, w_value, preferred_element_type=jnp.float32).reshape(
        row_count, head_count, head_size
    )
    decay_low = jnp.tanh(jnp.dot(tokens, decay_down, preferred_element_type=jnp.float32)).astype(
        jnp.bfloat16
    )
    decay_pre = decay_base + jnp.dot(decay_low, decay_up, preferred_element_type=jnp.float32)
    log_rate = -jax.nn.softplus(-decay_pre) - 0.5
    decay = jnp.exp(-jnp.exp(log_rate)).reshape(row_count, head_count, head_size)
    rate_low = jnp.dot(tokens, rate_down, preferred_element_type=jnp.float32).astype(jnp.bfloat16)
    in_rate = jax.nn.sigmoid(
        rate_base + jnp.dot(rate_low, rate_up, preferred_element_type=jnp.float32)
    ).reshape(row_count, head_count, head_size)
    unit_keys = key_vecs * lax.rsqrt(jnp.sum(key_vecs * key_vecs, -1, keepdims=True) + key_epsilon)
    removed = jnp.einsum("bhij,bhj->bhi", state, -unit_keys)
    updated = (
        state * decay[:, :, None, :]
        + removed[..., None] * (unit_keys * in_rate)[:, :, None, :]
        + value_vecs[..., None] * key_vecs[:, :, None, :]
    )
    read_out = jnp.einsum("bhij,bhj->bhi", updated, recep)
    centre = jnp.mean(read_out, -1, keepdims=True)
    spread = jnp.mean(jnp.square(read_out - centre), -1, keepdims=True)
    normed = ((read_out - centre) * lax.rsqrt(spread + head_epsilon)).reshape(
        row_count, head_count * head_size
    ) * head_gain
    return jnp.dot(normed.astype(jnp.bfloat16), w_out, preferred_element_type=jnp.float32)


def first_norm(values, gain):
    centre = jnp.mean(values, -1, keepdims=True)
    spread = jnp.mean(jnp.square(values - centre), -1, keepdims=True)
    return ((values - centre) * lax.rsqrt(spread + norm_epsilon) * gain).astype(jnp.bfloat16)


def route_tables(routes, route_weights, experts, capacity):
    expert_hits = (
        routes[:, :, None] == jnp.arange(experts, dtype=jnp.int32)[None, None, :]
    ).astype(jnp.int32)
    row_hits = jnp.sum(expert_hits, 1, dtype=jnp.int32)
    earlier = jnp.cumsum(row_hits, 0, dtype=jnp.int32) - row_hits
    slot_index = jnp.sum(earlier[:, None, :] * expert_hits, 2, dtype=jnp.int32)
    target = routes * capacity + slot_index
    places = jnp.arange(experts * capacity, dtype=jnp.int32)
    slot_match = target[:, :, None] == places[None, None, :]
    dispatch_tokens = jnp.any(slot_match, 1).astype(jnp.bfloat16)
    combine_experts = jnp.sum(jnp.where(slot_match, route_weights[:, :, None], 0.0), 1)
    return (dispatch_tokens, combine_experts)


def shards(
    tokens,
    state,
    w_recep,
    w_key,
    w_value,
    w_out,
    decay_base,
    decay_down,
    decay_up,
    rate_base,
    rate_down,
    rate_up,
    head_gain,
    first_gain,
    expert_gate,
    expert_up,
    expert_down,
    dense_gate,
    dense_up,
    dense_down,
    branch_gate,
    second_gain,
    routes,
    route_weights,
):
    row_count = tokens.shape[0]
    model_width = tokens.shape[1]
    quarter = w_recep.shape[1]
    tp_index = lax.axis_index("tp")
    partial_mix = time_mixer(
        tokens,
        state,
        w_recep,
        w_key,
        w_value,
        w_out,
        decay_base,
        decay_down,
        decay_up,
        rate_base,
        rate_down,
        rate_up,
        head_gain,
    )
    mixed = lax.psum(partial_mix, "tp")
    x_mid = first_norm(residual_scale * tokens.astype(jnp.float32) + mixed, first_gain)
    own_columns = lax.dynamic_slice_in_dim(x_mid, tp_index * quarter, quarter, 1)
    experts = lax.axis_size("ep") // SPLIT
    capacity = min(row_count, max(2, 2 * row_count * routes.shape[1] // experts))
    dispatch_tokens, combine_experts = route_tables(routes, route_weights, experts, capacity)
    packed_rows = lax.dot_general(
        dispatch_tokens, x_mid, (((0,), (0,)), ((), ())), preferred_element_type=jnp.float32
    ).astype(jnp.bfloat16)
    outgoing = jnp.repeat(packed_rows.reshape(experts, capacity, x_mid.shape[1]), SPLIT, axis=0)
    arrived = lax.all_to_all(outgoing, "ep", split_axis=0, concat_axis=0, tiled=True)
    sources = arrived.shape[0]
    slot_count = arrived.shape[1]
    flat_rows = arrived.reshape(sources * slot_count, model_width)
    gate_pre = jnp.dot(flat_rows, expert_gate[0], preferred_element_type=jnp.float32)
    up_pre = jnp.dot(flat_rows, expert_up[0], preferred_element_type=jnp.float32)
    hidden = (jax.nn.silu(gate_pre) * up_pre).astype(jnp.bfloat16)
    partial_out = jnp.dot(hidden, expert_down[0], preferred_element_type=jnp.float32).reshape(
        sources, slot_count, model_width
    )
    summed = lax.psum_scatter(
        partial_out.astype(jnp.bfloat16), "tp", scatter_dimension=2, tiled=True
    ).astype(jnp.float32)
    returned = lax.all_to_all(
        summed.astype(jnp.bfloat16), "ep", split_axis=0, concat_axis=0, tiled=True
    ).astype(summed.dtype)
    expert_out = jnp.sum(returned.reshape(experts, SPLIT, capacity, quarter), 1).reshape(
        experts * capacity, quarter
    )
    routed_part = jnp.dot(
        combine_experts,
        expert_out,
        precision=lax.Precision.HIGHEST,
        preferred_element_type=jnp.float32,
    )
    branch = jax.nn.sigmoid(jnp.dot(x_mid, branch_gate, preferred_element_type=jnp.float32))
    shard_rows = lax.all_gather(x_mid, "ep", axis=0, tiled=True)
    gate_pre = lax.dot_general(
        shard_rows, dense_gate, (((1,), (1,)), ((), ())), preferred_element_type=jnp.float32
    )
    up_pre = lax.dot_general(
        shard_rows, dense_up, (((1,), (1,)), ((), ())), preferred_element_type=jnp.float32
    )
    dense_hidden = (jax.nn.silu(gate_pre) * up_pre).astype(jnp.bfloat16)
    dense_part = lax.psum_scatter(
        jnp.dot(dense_hidden, dense_down, preferred_element_type=jnp.float32),
        "ep",
        scatter_dimension=0,
        tiled=True,
    )
    second_sum = (
        residual_scale * own_columns.astype(jnp.float32)
        + routed_part
        + branch[:, None] * dense_part
    )
    row_sums, square_sums = lax.psum(
        (jnp.sum(second_sum, 1), jnp.sum(second_sum * second_sum, 1)), "tp"
    )
    average = row_sums / model_width
    spread = square_sums / model_width - average * average
    return (
        (second_sum - average[:, None]) * lax.rsqrt(spread + norm_epsilon)[:, None] * second_gain
    ).astype(jnp.bfloat16)


def solution(mesh):
    return jax.shard_map(
        shards,
        mesh=mesh,
        in_specs=(
            P("ep", None),
            P("ep", "tp", None, None),
            P(None, "tp"),
            P(None, "tp"),
            P(None, "tp"),
            P("tp", None),
            P("tp"),
            P(),
            P(None, "tp"),
            P("tp"),
            P(),
            P(None, "tp"),
            P("tp"),
            P(),
            P("ep", None, "tp"),
            P("ep", None, "tp"),
            P("ep", "tp", None),
            P("ep", None),
            P("ep", None),
            P("ep", "tp"),
            P(),
            P("tp"),
            P("ep", None),
            P("ep", None),
        ),
        out_specs=P("ep", "tp"),
        check_vma=False,
    )
```

profile of v0, /device:TPU:0, one launch (start us, length us, event | category | flops | bytes accessed | tf_op | source)
XLA Modules:
  0.0 162.2 jit_solution(11377209794120408051)
XLA Ops:
  6.5 1.6 fusion.56
  8.3 1.2 fusion.32
  9.6 1.5 fusion.59
  11.2 1.3 fusion.49
  12.6 1.5 fusion.58
  14.2 3.5 %fusion.57 = f32[16,8,1,64]{3,2,1,0:T(1,128)S(1)} fusion(f32[16,8,64,1]{2,3,1,0:T(1,128)S(1)} %bitcast.81, f32[16,8,64,64]{3,2,1,0:T(8,128)} %param.25), kind=kOutput, calls=%fused_computation.85 | convolution fusion | flops 1048576 | bytes 2162688 | tf_op jit(solution)/shard_map/bhij,bhj->bhi/dot_general | solution.py:51
  17.8 2.9 %fusion = f32[16,8,1,64]{3,2,1,0:T(1,128)S(1)} fusion(f32[16,8,64,1]{2,3,1,0:T(1,128)S(1)} %bitcast.83, f32[16,8,64,64]{3,2,1,0:T(8,128)S(1)} %copy-done.1, f32[16,8,64]{2,1,0:T(8,128)S(1)} %reshape.96, f32[16,8,64]{2,1,0:T(8,128)S(1)} %mul.177, f32[16,8,64]{2,1,0:T(8,128)S(1)} %get-tuple-element.10, f32[16,8,64]{2,1,0:T(8,128)S(1)} %bitcast.82, ...), kind=kOutput, calls=%fused_computation | convolution fusion | flops 3670016 | bytes 2326528 | tf_op jit(solution)/shard_map/bhij,bhj->bhi/dot_general | solution.py:57
  21.2 2.1 %fusion.51 = f32[16,1024]{1,0:T(8,128)} fusion(bf16[512,1024]{1,0:T(8,128)(2,1)} %param.29, f32[16,512]{1,0:T(8,128)S(1)} %reshape.99, f32[512]{0:T(512)S(1)} %copy-done.7), kind=kOutput, calls=%fused_computation.66 | convolution fusion | flops 16793600 | bytes 1148928 | tf_op jit(solution)/shard_map/dot_general | solution.py:63
  23.7 23.4 %all-reduce.3.cloned.1.call-done = f32[16,1024]{1,0:T(8,128)} async-done(((f32[16,1024]{1,0:T(8,128)}), f32[16,1024]{1,0:T(8,128)}) %all-reduce.3.cloned.1.call-update) | async-done | bytes 65552 | tf_op jit(solution)/shard_map/psum | solution.py:132
  47.2 1.1 fusion.50
  48.2 1.0 multiply_reduce_fusion
  49.3 0.9 multiply_convert_fusion
  50.5 19.7 %all_to_all.10 = bf16[16,16,1024]{2,1,0:T(8,128)(2,1)S(1)} all-to-all(bf16[16,16,1024]{2,1,0:T(8,128)(2,1)S(1)} %bitcast.72), channel_id=1, replica_groups=mesh['ep'=16,'tp'=2] {'ep'}, dimensions={0} | all-to-all | bytes 1048576 | tf_op jit(solution)/shard_map/all_to_all | solution.py:142
  70.2 0.6 fusion.15
  70.8 0.6 fusion.23
  71.6 1.4 fusion.17
  73.1 21.3 %all_gather.3 = bf16[256,1024]{1,0:T(8,128)(2,1)S(1)} all-gather(bf16[16,1024]{1,0:T(8,128)(2,1)S(1)} %multiply_convert_fusion), channel_id=1, replica_groups=mesh['ep'=16,'tp'=2] {'ep'}, dimensions={0}, use_global_device_ids=true | all-gather | bytes 557056 | tf_op jit(solution)/shard_map/all_gather | solution.py:168
  94.8 1.5 fusion.27
  96.3 3.5 %all-to-all-start.1 = ((bf16[16,16,512]{2,1,0:T(8,128)(2,1)}), bf16[16,16,512]{2,1,0:T(8,128)(2,1)S(1)}, u32[]{:S(2)}, u32[]{:S(2)}) async-start(bf16[16,16,512]{2,1,0:T(8,128)(2,1)} %reduce-scatter.3.cloned.1.call-done), calls=%async_computation.2 | async-start | bytes 524288 | tf_op jit(solution)/shard_map/all_to_all | solution.py:155
  100.1 9.7 %all-to-all-done.1 = bf16[16,16,512]{2,1,0:T(8,128)(2,1)S(1)} async-done(((bf16[16,16,512]{2,1,0:T(8,128)(2,1)}), bf16[16,16,512]{2,1,0:T(8,128)(2,1)S(1)}, u32[]{:S(2)}, u32[]{:S(2)}) %all-to-all-start.1) | async-done | bytes 262176 | tf_op jit(solution)/shard_map/all_to_all | solution.py:155
  109.9 39.1 %reduce-scatter.5.cloned.1.call-done = f32[16,512]{1,0:T(8,128)} async-done(((f32[256,512]{1,0:T(8,128)}), f32[16,512]{1,0:T(8,128)}) %reduce-scatter.5.cloned.1.call-update) | async-done | bytes 32784 | tf_op jit(solution)/shard_map/reduce_scatter | solution.py:176
  148.9 1.1 fusion.55
  150.0 4.9 %all-reduce = (f32[16]{0:T(128)S(1)}, f32[16]{0:T(128)S(1)}) all-reduce(f32[16]{0:T(128)S(1)} %get-tuple-element.6, f32[16]{0:T(128)S(1)} %get-tuple-element.5), channel_id=1, replica_groups=mesh['ep'=16,'tp'=2] {'tp'}, use_global_device_ids=true, to_apply=%region_17.18 | all-reduce | flops 32 | bytes 256 | tf_op jit(solution)/shard_map/psum | solution.py:187
  154.9 0.7 multiply_convert_fusion.1
  (68 shorter events, 2.7 us)
Async XLA Ops:
  6.5 65.1 %copy-start = (bf16[1,704,1024]{2,1,0:T(8,128)(2,1)S(1)}, bf16[1,704,1024]{2,1,0:T(8,128)(2,1)}, u32[]{:S(2)}) copy-start(bf16[1,704,1024]{2,1,0:T(8,128)(2,1)} %param.40) | copy-start | bytes 4325380
  6.5 40.6 %all-reduce.3.cloned.1.call-start = ((), (), s32[]{:S(2)}) async-start(), calls=%async_computation.4 | async-start | bytes 131072 | tf_op jit(solution)/shard_map/psum | solution.py:132
  14.1 3.6 %copy-start.1 = (f32[16,8,64,64]{3,2,1,0:T(8,128)S(1)}, f32[16,8,64,64]{3,2,1,0:T(8,128)}, u32[]{:S(2)}) copy-start(f32[16,8,64,64]{3,2,1,0:T(8,128)} %param.25) | copy-start | bytes 6291460
  17.7 3.5 %copy-start.7 = (f32[512]{0:T(512)S(1)}, f32[512]{0:T(512)}, u32[]{:S(2)}) copy-start(f32[512]{0:T(512)} %param.36) | copy-start | bytes 6148
  17.7 5.6 %copy-start.5 = (s32[16,2]{0,1:T(2,128)S(1)}, s32[16,2]{0,1:T(2,128)}, u32[]{:S(2)}) copy-start(s32[16,2]{0,1:T(2,128)} %param.46) | copy-start | bytes 388
  17.7 29.4 %copy-start.2 = (bf16[16,1024]{1,0:T(8,128)(2,1)S(1)}, bf16[16,1024]{1,0:T(8,128)(2,1)}, u32[]{:S(2)}) copy-start(bf16[16,1024]{1,0:T(8,128)(2,1)} %param.24) | copy-start | bytes 98308
  17.8 31.5 %copy-start.6 = (f32[1024]{0:T(1024)S(1)}, f32[1024]{0:T(1024)}, u32[]{:S(2)}) copy-start(f32[1024]{0:T(1024)} %param.37) | copy-start | bytes 12292
  17.8 52.4 %copy-start.3 = (bf16[1,1024,704]{1,2,0:T(8,128)(2,1)S(1)}, bf16[1,1024,704]{1,2,0:T(8,128)(2,1)}, u32[]{:S(2)}) copy-start(bf16[1,1024,704]{1,2,0:T(8,128)(2,1)} %param.38) | copy-start | bytes 4325380
  23.3 73.0 %reduce-scatter.3.cloned.1.call-start = ((), (), s32[]{:S(2)}) async-start(), calls=%async_computation.5 | async-start | bytes 786432 | tf_op jit(solution)/shard_map/reduce_scatter | solution.py:152
  47.2 23.6 %copy-start.11 = (bf16[1,1024,704]{1,2,0:T(8,128)(2,1)S(1)}, bf16[1,1024,704]{1,2,0:T(8,128)(2,1)}, u32[]{:S(2)}) copy-start(bf16[1,1024,704]{1,2,0:T(8,128)(2,1)} %param.39) | copy-start | bytes 4325380
  70.8 23.6 %copy-start.4 = (bf16[176,1024]{1,0:T(8,128)(2,1)S(1)}, bf16[176,1024]{1,0:T(8,128)(2,1)}, u32[]{:S(2)}) copy-start(bf16[176,1024]{1,0:T(8,128)(2,1)} %param.41) | copy-start | bytes 1081348
  70.8 23.9 %copy-start.12 = (bf16[176,1024]{1,0:T(8,128)(2,1)S(1)}, bf16[176,1024]{1,0:T(8,128)(2,1)}, u32[]{:S(2)}) copy-start(bf16[176,1024]{1,0:T(8,128)(2,1)} %param.42) | copy-start | bytes 1081348
  70.8 23.9 %copy-start.13 = (bf16[176,512]{1,0:T(8,128)(2,1)S(1)}, bf16[176,512]{1,0:T(8,128)(2,1)}, u32[]{:S(2)}) copy-start(bf16[176,512]{1,0:T(8,128)(2,1)} %param.43) | copy-start | bytes 540676
  71.4 28.4 %copy-start.8 = (bf16[1024]{0:T(1024)(128)(2,1)S(1)}, bf16[1024]{0:T(1024)(128)(2,1)}, u32[]{:S(2)}) copy-start(bf16[1024]{0:T(1024)(128)(2,1)} %param.44) | copy-start | bytes 6148
  71.4 28.4 %copy-start.10 = (f32[16,2]{0,1:T(2,128)S(1)}, f32[16,2]{0,1:T(2,128)}, u32[]{:S(2)}) copy-start(f32[16,2]{0,1:T(2,128)} %param.47) | copy-start | bytes 388
  71.6 83.3 %copy-start.9 = (f32[512]{0:T(512)S(1)}, f32[512]{0:T(512)}, u32[]{:S(2)}) copy-start(f32[512]{0:T(512)} %param.45) | copy-start | bytes 6148
  73.1 75.9 %reduce-scatter.5.cloned.1.call-start = ((), (), s32[]{:S(2)}) async-start(), calls=%async_computation.6 | async-start | bytes 557056 | tf_op jit(solution)/shard_map/reduce_scatter | solution.py:176
  96.3 13.5 %all-to-all-start.1 = ((bf16[16,16,512]{2,1,0:T(8,128)(2,1)}), bf16[16,16,512]{2,1,0:T(8,128)(2,1)S(1)}, u32[]{:S(2)}, u32[]{:S(2)}) async-start(bf16[16,16,512]{2,1,0:T(8,128)(2,1)} %reduce-scatter.3.cloned.1.call-done), calls=%async_computation.2 | async-start | bytes 524288 | tf_op jit(solution)/shard_map/all_to_all | solution.py:155
Sparse Core Ops, SparseCore 0:
  23.4 23.6 all-reduce.2
  73.2 13.2 reduce-scatter.2
  96.4 52.5 reduce-scatter.4
where the time goes:
time: 163 us; the launch traced here: 162 us
  waiting for transfers between devices  72.3 us (44%)
  blocking collectives  45.9 us (28%)
  matrix products  21.3 us (13%)
  between operations  13.4 us (8%)
  other arithmetic  4.56 us (3%)
  starting transfers between devices  3.63 us (2%)
    reduce_scatter x1, waiting for transfers between devices, shards(): lax.psum_scatter(jnp.dot(dense_hidden, dense_down, preferred_element_type...  39.1 us
    psum x1, waiting for transfers between devices, shards(): mixed = lax.psum(partial_mix, 'tp')  23.4 us
    all_gather x1, blocking collectives, shards(): shard_rows = lax.all_gather(x_mid, 'ep', axis=0, tiled=True)  21.3 us
    all_to_all x1, blocking collectives, shards(): lax.all_to_all(outgoing, 'ep', split_axis=0, concat_axis=0, tiled=True)  19.7 us
    all_to_all x1, waiting for transfers between devices, shards(): lax.all_to_all(summed.astype(jnp.bfloat16), 'ep', split_axis=0, concat_ax...  9.73 us
    psum x1, blocking collectives, shards(): lax.psum((jnp.sum(second_sum, 1), jnp.sum(second_sum * second_sum, 1)), '...  4.93 us
    all_to_all x1, starting transfers between devices, shards(): lax.all_to_all(summed.astype(jnp.bfloat16), 'ep', split_axis=0, concat_ax...  3.54 us
    dot_general x1, matrix products, time_mixer(): removed = jnp.einsum('bhij,bhj->bhi', state, -unit_keys)  3.51 us
  transfers between devices with their start and end apart: 4, of which 3 were waited for; matrix products, arithmetic and copies ran while one was open for 1% of the time, Pallas kernels for 0%

commit v1 on v0

--- a/solution.py
+++ b/solution.py
@@ -8,6 +8,11 @@
 norm_epsilon = 1e-05
 head_epsilon = 0.00064
 key_epsilon = 1e-06
+
+
+def gather_and_add(block, axis):
+    parts = lax.all_gather(block, axis)
+    return jnp.sum(parts, axis=0)
 
 
 def time_mixer(
@@ -129,7 +134,7 @@
         rate_up,
         head_gain,
     )
-    mixed = lax.psum(partial_mix, "tp")
+    mixed = gather_and_add(partial_mix, "tp")
     x_mid = first_norm(residual_scale * tokens.astype(jnp.float32) + mixed, first_gain)
     own_columns = lax.dynamic_slice_in_dim(x_mid, tp_index * quarter, quarter, 1)
     experts = lax.axis_size("ep") // SPLIT

time: 163 us -> 144 us (0.88)
  waiting for transfers between devices: 72.3 us -> 49.8 us
  blocking collectives: 45.9 us -> 52.6 us
  other arithmetic: 4.56 us -> 1.94 us
    psum x1 -> x0, waiting for transfers between devices: 23.4 us -> none  [shards(): mixed = lax.psum(partial_mix, 'tp')]
    all_gather x0 -> x1, blocking collectives: none -> 5.88 us  [gather_and_add(): parts = lax.all_gather(block, axis)]
  transfers between devices with their start and end apart: 4 -> 3, of which waited for: 3 -> 2; matrix products, arithmetic and copies ran while one was open for 1% -> 1% of each run, Pallas kernels for 0% -> 0%
where the time goes in v1:
time: 144 us; the launch traced here: 143 us
  blocking collectives  52.6 us (37%)
  waiting for transfers between devices  49.8 us (35%)
  matrix products  20.7 us (14%)
  between operations  13.7 us (10%)
  starting transfers between devices  3.59 us (2%)
  other arithmetic  1.94 us (1%)
    reduce_scatter x1, waiting for transfers between devices, shards(): lax.psum_scatter(jnp.dot(dense_hidden, dense_down, preferred_element_type...  40.1 us
    all_gather x1, blocking collectives, shards(): shard_rows = lax.all_gather(x_mid, 'ep', axis=0, tiled=True)  21.3 us
    all_to_all x1, blocking collectives, shards(): lax.all_to_all(outgoing, 'ep', split_axis=0, concat_axis=0, tiled=True)  20.5 us
    all_to_all x1, waiting for transfers between devices, shards(): lax.all_to_all(summed.astype(jnp.bfloat16), 'ep', split_axis=0, concat_ax...  9.73 us
    all_gather x1, blocking collectives, gather_and_add(): parts = lax.all_gather(block, axis)  5.88 us
    psum x1, blocking collectives, shards(): lax.psum((jnp.sum(second_sum, 1), jnp.sum(second_sum * second_sum, 1)), '...  4.93 us
    all_to_all x1, starting transfers between devices, shards(): lax.all_to_all(summed.astype(jnp.bfloat16), 'ep', split_axis=0, concat_ax...  3.55 us
    dot_general x1, matrix products, time_mixer(): removed = jnp.einsum('bhij,bhj->bhi', state, -unit_keys)  3.51 us
  transfers between devices with their start and end apart: 3, of which 2 were waited for; matrix products, arithmetic and copies ran while one was open for 1% of the time, Pallas kernels for 0%

profile of v1, /device:TPU:0, one launch (start us, length us, event | category | flops | bytes accessed | tf_op | source)
XLA Modules:
  0.0 143.4 jit_solution(1426825693756930415)
XLA Ops:
  6.5 1.6 %fusion.56 = f32[16,512]{1,0:T(8,128)S(1)} fusion(bf16[16,1024]{1,0:T(8,128)(2,1)} %param.24, bf16[1024,512]{1,0:T(8,128)(2,1)} %param.27), kind=kOutput, calls=%fused_computation.84 | convolution fusion | flops 16777216 | bytes 1114112 | tf_op jit(solution)/shard_map/dot_general | solution.py:39
  8.3 1.2 fusion.32
  9.6 1.5 %fusion.59 = f32[16,512]{1,0:T(8,128)S(1)} fusion(bf16[16,1024]{1,0:T(8,128)(2,1)} %param.24, bf16[1024,512]{1,0:T(8,128)(2,1)} %param.26), kind=kOutput, calls=%fused_computation.87 | convolution fusion | flops 16777216 | bytes 1114112 | tf_op jit(solution)/shard_map/dot_general | solution.py:36
  11.2 1.3 fusion.49
  12.6 1.5 %fusion.58 = f32[16,512]{1,0:T(8,128)S(1)} fusion(bf16[16,1024]{1,0:T(8,128)(2,1)} %param.24, bf16[1024,512]{1,0:T(8,128)(2,1)} %param.28), kind=kOutput, calls=%fused_computation.86 | convolution fusion | flops 16777216 | bytes 1114112 | tf_op jit(solution)/shard_map/dot_general | solution.py:42
  14.2 3.5 %fusion.57 = f32[16,8,1,64]{3,2,1,0:T(1,128)S(1)} fusion(f32[16,8,64,1]{2,3,1,0:T(1,128)S(1)} %bitcast.83, f32[16,8,64,64]{3,2,1,0:T(8,128)} %param.25), kind=kOutput, calls=%fused_computation.85 | convolution fusion | flops 1048576 | bytes 2162688 | tf_op jit(solution)/shard_map/bhij,bhj->bhi/dot_general | solution.py:56
  17.8 2.9 %fusion = f32[16,8,1,64]{3,2,1,0:T(1,128)S(1)} fusion(f32[16,8,64,1]{2,3,1,0:T(1,128)S(1)} %bitcast.85, f32[16,8,64,64]{3,2,1,0:T(8,128)S(1)} %copy-done.1, f32[16,8,64]{2,1,0:T(8,128)S(1)} %reshape.96, f32[16,8,64]{2,1,0:T(8,128)S(1)} %mul.177, f32[16,8,64]{2,1,0:T(8,128)S(1)} %get-tuple-element.10, f32[16,8,64]{2,1,0:T(8,128)S(1)} %bitcast.84, ...), kind=kOutput, calls=%fused_computation | convolution fusion | flops 3670016 | bytes 2326528 | tf_op jit(solution)/shard_map/bhij,bhj->bhi/dot_general | solution.py:62
  21.2 1.5 %fusion.51 = f32[16,1024]{1,0:T(8,128)S(1)} fusion(bf16[512,1024]{1,0:T(8,128)(2,1)} %param.29, f32[16,512]{1,0:T(8,128)S(1)} %reshape.99, f32[512]{0:T(512)S(1)} %copy-done.7), kind=kOutput, calls=%fused_computation.66 | convolution fusion | flops 16793600 | bytes 1148928 | tf_op jit(solution)/shard_map/dot_general | solution.py:68
  22.7 5.9 %all-gather = f32[32,1024]{1,0:T(8,128)S(1)} all-gather(f32[16,1024]{1,0:T(8,128)S(1)} %fusion.51), channel_id=2, replica_groups=mesh['ep'=16,'tp'=2] {'tp'}, dimensions={0}, use_global_device_ids=true | all-gather | bytes 196608 | tf_op jit(solution)/shard_map/all_gather | solution.py:14
  28.7 0.2 multiply_reduce_fusion
  29.4 0.2 convolution_convert_fusion
  29.7 20.5 %all_to_all.10 = bf16[16,16,1024]{2,1,0:T(8,128)(2,1)S(1)} all-to-all(bf16[16,16,1024]{2,1,0:T(8,128)(2,1)S(1)} %bitcast.73), channel_id=1, replica_groups=mesh['ep'=16,'tp'=2] {'ep'}, dimensions={0} | all-to-all | bytes 1048576 | tf_op jit(solution)/shard_map/all_to_all | solution.py:147
  50.2 0.6 fusion.15
  50.8 0.6 fusion.23
  51.6 1.4 fusion.17
  53.1 21.3 %all_gather.11 = bf16[256,1024]{1,0:T(8,128)(2,1)S(1)} all-gather(bf16[16,1024]{1,0:T(8,128)(2,1)S(1)} %multiply_convert_fusion), channel_id=1, replica_groups=mesh['ep'=16,'tp'=2] {'ep'}, dimensions={0}, use_global_device_ids=true | all-gather | bytes 557056 | tf_op jit(solution)/shard_map/all_gather | solution.py:173
  74.4 0.3 fusion.60
  74.7 1.5 %fusion.27 = f32[256,512]{1,0:T(8,128)} fusion(bf16[176,512]{1,0:T(8,128)(2,1)S(1)} %copy-done.13, bf16[256,1024]{1,0:T(8,128)(2,1)S(1)} %all_gather.11, bf16[176,1024]{1,0:T(8,128)(2,1)S(1)} %copy-done.12, f32[256,176]{0,1:T(8,128)S(1)} %fusion.60), kind=kOutput, calls=%fused_computation.23 | convolution fusion | flops 138682368 | bytes 1769472 | tf_op jit(solution)/shard_map/dot_general | solution.py:182
  76.2 3.5 %all-to-all-start.1 = ((bf16[16,16,512]{2,1,0:T(8,128)(2,1)}), bf16[16,16,512]{2,1,0:T(8,128)(2,1)S(1)}, u32[]{:S(2)}, u32[]{:S(2)}) async-start(bf16[16,16,512]{2,1,0:T(8,128)(2,1)} %reduce-scatter.3.cloned.1.call-done), calls=%async_computation.2 | async-start | bytes 524288 | tf_op jit(solution)/shard_map/all_to_all | solution.py:160
  80.0 9.7 %all-to-all-done.1 = bf16[16,16,512]{2,1,0:T(8,128)(2,1)S(1)} async-done(((bf16[16,16,512]{2,1,0:T(8,128)(2,1)}), bf16[16,16,512]{2,1,0:T(8,128)(2,1)S(1)}, u32[]{:S(2)}, u32[]{:S(2)}) %all-to-all-start.1) | async-done | bytes 262176 | tf_op jit(solution)/shard_map/all_to_all | solution.py:160
  89.8 40.1 %reduce-scatter.5.cloned.1.call-done = f32[16,512]{1,0:T(8,128)} async-done(((f32[256,512]{1,0:T(8,128)}), f32[16,512]{1,0:T(8,128)}) %reduce-scatter.5.cloned.1.call-update) | async-done | bytes 32784 | tf_op jit(solution)/shard_map/reduce_scatter | solution.py:181
  129.9 1.1 fusion.55
  130.9 4.9 %all-reduce = (f32[16]{0:T(128)S(1)}, f32[16]{0:T(128)S(1)}) all-reduce(f32[16]{0:T(128)S(1)} %get-tuple-element.6, f32[16]{0:T(128)S(1)} %get-tuple-element.5), channel_id=1, replica_groups=mesh['ep'=16,'tp'=2] {'tp'}, use_global_device_ids=true, to_apply=%region_17.18 | all-reduce | flops 32 | bytes 256 | tf_op jit(solution)/shard_map/psum | solution.py:192
  135.9 0.7 multiply_convert_fusion.1
  (67 shorter events, 2.3 us)
Async XLA Ops:
  6.5 45.1 %copy-start = (bf16[1,704,1024]{2,1,0:T(8,128)(2,1)S(1)}, bf16[1,704,1024]{2,1,0:T(8,128)(2,1)}, u32[]{:S(2)}) copy-start(bf16[1,704,1024]{2,1,0:T(8,128)(2,1)} %param.40) | copy-start | bytes 4325380
  6.5 69.7 %reduce-scatter.3.cloned.1.call-start = ((), (), s32[]{:S(2)}) async-start(), calls=%async_computation.4 | async-start | bytes 786432 | tf_op jit(solution)/shard_map/reduce_scatter | solution.py:157
  14.1 3.6 %copy-start.1 = (f32[16,8,64,64]{3,2,1,0:T(8,128)S(1)}, f32[16,8,64,64]{3,2,1,0:T(8,128)}, u32[]{:S(2)}) copy-start(f32[16,8,64,64]{3,2,1,0:T(8,128)} %param.25) | copy-start | bytes 6291460
  17.7 3.5 %copy-start.7 = (f32[512]{0:T(512)S(1)}, f32[512]{0:T(512)}, u32[]{:S(2)}) copy-start(f32[512]{0:T(512)} %param.36) | copy-start | bytes 6148
  17.7 10.8 %copy-start.2 = (bf16[16,1024]{1,0:T(8,128)(2,1)S(1)}, bf16[16,1024]{1,0:T(8,128)(2,1)}, u32[]{:S(2)}) copy-start(bf16[16,1024]{1,0:T(8,128)(2,1)} %param.24) | copy-start | bytes 98308
  17.8 11.2 %copy-start.5 = (s32[16,2]{0,1:T(2,128)S(1)}, s32[16,2]{0,1:T(2,128)}, u32[]{:S(2)}) copy-start(s32[16,2]{0,1:T(2,128)} %param.46) | copy-start | bytes 388
  17.8 11.5 %copy-start.6 = (f32[1024]{0:T(1024)S(1)}, f32[1024]{0:T(1024)}, u32[]{:S(2)}) copy-start(f32[1024]{0:T(1024)} %param.37) | copy-start | bytes 12292
  17.8 32.4 %copy-start.3 = (bf16[1,1024,704]{1,2,0:T(8,128)(2,1)S(1)}, bf16[1,1024,704]{1,2,0:T(8,128)(2,1)}, u32[]{:S(2)}) copy-start(bf16[1,1024,704]{1,2,0:T(8,128)(2,1)} %param.38) | copy-start | bytes 4325380
  29.2 21.6 %copy-start.11 = (bf16[1,1024,704]{1,2,0:T(8,128)(2,1)S(1)}, bf16[1,1024,704]{1,2,0:T(8,128)(2,1)}, u32[]{:S(2)}) copy-start(bf16[1,1024,704]{1,2,0:T(8,128)(2,1)} %param.39) | copy-start | bytes 4325380
  50.8 23.6 %copy-start.4 = (bf16[176,1024]{1,0:T(8,128)(2,1)S(1)}, bf16[176,1024]{1,0:T(8,128)(2,1)}, u32[]{:S(2)}) copy-start(bf16[176,1024]{1,0:T(8,128)(2,1)} %param.41) | copy-start | bytes 1081348
  50.8 23.9 %copy-start.12 = (bf16[176,1024]{1,0:T(8,128)(2,1)S(1)}, bf16[176,1024]{1,0:T(8,128)(2,1)}, u32[]{:S(2)}) copy-start(bf16[176,1024]{1,0:T(8,128)(2,1)} %param.42) | copy-start | bytes 1081348
  50.8 23.9 %copy-start.13 = (bf16[176,512]{1,0:T(8,128)(2,1)S(1)}, bf16[176,512]{1,0:T(8,128)(2,1)}, u32[]{:S(2)}) copy-start(bf16[176,512]{1,0:T(8,128)(2,1)} %param.43) | copy-start | bytes 540676
  51.4 28.4 %copy-start.8 = (bf16[1024]{0:T(1024)(128)(2,1)S(1)}, bf16[1024]{0:T(1024)(128)(2,1)}, u32[]{:S(2)}) copy-start(bf16[1024]{0:T(1024)(128)(2,1)} %param.44) | copy-start | bytes 6148
  51.4 28.4 %copy-start.10 = (f32[16,2]{0,1:T(2,128)S(1)}, f32[16,2]{0,1:T(2,128)}, u32[]{:S(2)}) copy-start(f32[16,2]{0,1:T(2,128)} %param.47) | copy-start | bytes 388
  51.6 84.3 %copy-start.9 = (f32[512]{0:T(512)S(1)}, f32[512]{0:T(512)}, u32[]{:S(2)}) copy-start(f32[512]{0:T(512)} %param.45) | copy-start | bytes 6148
  53.0 76.9 %reduce-scatter.5.cloned.1.call-start = ((), (), s32[]{:S(2)}) async-start(), calls=%async_computation.5 | async-start | bytes 557056 | tf_op jit(solution)/shard_map/reduce_scatter | solution.py:181
  76.2 13.5 %all-to-all-start.1 = ((bf16[16,16,512]{2,1,0:T(8,128)(2,1)}), bf16[16,16,512]{2,1,0:T(8,128)(2,1)S(1)}, u32[]{:S(2)}, u32[]{:S(2)}) async-start(bf16[16,16,512]{2,1,0:T(8,128)(2,1)} %reduce-scatter.3.cloned.1.call-done), calls=%async_computation.2 | async-start | bytes 524288 | tf_op jit(solution)/shard_map/all_to_all | solution.py:160
Sparse Core Ops, SparseCore 0:
  53.1 14.1 reduce-scatter.2
  76.3 53.4 reduce-scatter.4
